TPU v7x, 512 devices: a whole 4x8x8 slice. The times are simulated.
512 devices in a mesh: sp: 32 (over z, x), tp: 16 (over y, core).
Axes of the slice: x: 4, y: 8, z: 8, core: 2. Of those that a mesh axis runs over, the one named last changes fastest.
Arguments:
- queries: bfloat16 [8192, 1024], P('sp', 'tp'), may hold values from -64 to 64
- keys: bfloat16 [8192, 1024], P('sp', 'tp'), may hold values from -64 to 64
- values: bfloat16 [8192, 1024], P('sp', 'tp'), may hold values from -6 to 6
- cum_gate: float32 [16, 8192], P('tp'), may hold values from -8192 to 0, as said below
- out_weight: bfloat16 [1024, 2048], P('tp'), may hold values from -0.375 to 0.375
- resid: bfloat16 [8192, 2048], P('sp'), may hold values from -6 to 6
- norm_gain: float32 [2048], replicated, may hold values from 0.1 to 1.9
- routes: int32 [8192, 2], P('sp'), may hold values from 0 to 31, all different within a row; in each aligned block of 256 rows (0 to 255, 256 to 511, ...) at most 20 rows name the same one
- route_weight: float32 [8192, 2], P('sp'), may hold values from 0.1 to 0.9
- gate_weight: bfloat16 [32, 2048, 4096], P('sp', None, 'tp'), may hold values from -0.125 to 0.125
- up_weight: bfloat16 [32, 2048, 4096], P('sp', None, 'tp'), may hold values from -0.125 to 0.125
- down_weight: bfloat16 [32, 4096, 2048], P('sp', 'tp'), may hold values from -0.09375 to 0.09375
Outputs:
- layer_out: bfloat16 [8192, 2048], P('sp', 'tp')
Inputs may be any that keep to these rules, and one draw needn't show every extreme that they name: `routes`: each token names 2 different experts. Among the rows of one index of sp, no expert is named more than 20 times, a bound that some block reaches. `cum_gate`: each head's row does not rise along the positions.
All inputs are finite; a program needn't handle non-finite values.
Results may differ from a plain program's by a relative error of at most 0.015.
Values may be sent and summed in bfloat16 or wider, within the bound.
No kernel may reach another device: no remote copies, remote signals or barrier semaphores. Data moves between devices by JAX's collectives and lax.ppermute only.
A program may use at most 64 MiB of HBM per device.

v0:
```python
import math
import jax
import jax.numpy as jnp
from jax import lax
from jax.sharding import PartitionSpec as P

HD = 64
epsilon = 1e-06


def in_one_piece(arrays, axis, dim, along):
    ends, at = ([], 0)
    for a in arrays[:-1]:
        at += a.shape[along]
        ends.append(at)
    both = jnp.concatenate(arrays, axis=along)
    return tuple(jnp.split(lax.all_gather(both, axis, axis=dim, tiled=True), ends, axis=along))


def in_blocks(x, dim, length):
    before, after = (x.shape[:dim], x.shape[dim + 1 :])
    return jnp.moveaxis(x.reshape(*before, length, -1, *after), dim, 0)


def sum_at_owner(x, axis, dim):
    tiles = in_blocks(x, dim, lax.axis_size(axis))
    arrived = lax.all_to_all(tiles, axis, split_axis=0, concat_axis=0, tiled=True)
    return arrived.astype(jnp.float32).sum(axis=0)


def from_everyone(x, axis):
    length = lax.axis_size(axis)
    return lax.all_to_all(jnp.broadcast_to(x[None], (length, *x.shape)), axis, 0, 0, tiled=True)


def of_everyone(x, axis):
    everything = from_everyone(x, axis)
    return jnp.sum(everything, axis=0)


def attend_block(
    carried, query_heads, cum_query, key_rows, value_rows, cum_keys, query_first, key_first
):
    best_score, weight_sum, value_sum = carried
    score_scale = query_heads.shape[-1] ** (-0.5)
    scores = (
        jnp.einsum("hqd,hkd->hqk", query_heads, key_rows, preferred_element_type=jnp.float32)
        * score_scale
    )
    scores = scores + cum_query[:, :, None] - cum_keys[:, None, :]
    query_pos = query_first + jnp.arange(query_heads.shape[1], dtype=jnp.int32)
    key_pos = key_first + jnp.arange(key_rows.shape[1], dtype=jnp.int32)
    permitted_mask = (key_pos[None, :] <= query_pos[:, None])[None]
    new_best = jnp.maximum(
        best_score, jnp.max(jnp.where(permitted_mask, scores, -jnp.inf), axis=-1)
    )
    weights = jnp.where(permitted_mask, jnp.exp(scores - new_best[..., None]), 0.0)
    shrink = jnp.exp(best_score - new_best)
    weight_sum = weight_sum * shrink + jnp.sum(weights, axis=-1)
    value_sum = value_sum * shrink[..., None] + jnp.einsum(
        "hqk,hkd->hqd", weights.astype(jnp.bfloat16), value_rows, preferred_element_type=jnp.float32
    )
    return (new_best, weight_sum, value_sum)


def local(
    queries,
    keys,
    values,
    cum_gate,
    out_weight,
    resid,
    norm_gain,
    routes,
    route_weight,
    gate_weight,
    up_weight,
    down_weight,
):
    rows_here = queries.shape[0]
    heads_here = queries.shape[1] // HD
    sp_count = lax.axis_size("sp")
    tp_count = lax.axis_size("tp")
    shift_amount = lax.axis_index("sp") * rows_here
    model_width = resid.shape[1]
    columns = model_width // tp_count
    column_first = lax.axis_index("tp") * columns
    query_heads = queries.reshape(rows_here, heads_here, HD).transpose(1, 0, 2)
    cum_query = lax.dynamic_slice_in_dim(cum_gate, shift_amount, rows_here, 1)
    start_state = (
        jnp.full((heads_here, rows_here), -1e30, jnp.float32),
        jnp.zeros((heads_here, rows_here), jnp.float32),
        jnp.zeros((heads_here, rows_here, HD), jnp.float32),
    )
    key_part, value_part = in_one_piece((keys, values), "sp", 0, 1)
    piece_rows = key_part.shape[0]
    key_block = math.gcd(piece_rows, 1024)

    def attend_piece(running):

        def key_step(block_index, inner_state):
            block_first = block_index * key_block
            key_rows = lax.dynamic_slice_in_dim(key_part, block_first, key_block, 0)
            key_rows = key_rows.reshape(key_block, heads_here, HD).transpose(1, 0, 2)
            value_rows = lax.dynamic_slice_in_dim(value_part, block_first, key_block, 0)
            value_rows = value_rows.reshape(key_block, heads_here, HD).transpose(1, 0, 2)
            cum_keys = lax.dynamic_slice_in_dim(cum_gate, block_first, key_block, 1)
            return attend_block(
                inner_state,
                query_heads,
                cum_query,
                key_rows,
                value_rows,
                cum_keys,
                shift_amount,
                block_first,
            )

        return lax.fori_loop(0, piece_rows // key_block, key_step, running)

    best_score, weight_sum, value_sum = lax.cond(
        jnp.int32(0) <= shift_amount + rows_here - 1,
        attend_piece,
        lambda running: running,
        start_state,
    )
    attended = (value_sum / weight_sum[..., None]).astype(jnp.bfloat16)
    attended = attended.transpose(1, 0, 2).reshape(rows_here, heads_here * HD)
    partial_value = jnp.dot(attended, out_weight, preferred_element_type=jnp.float32)
    mixed_sum = sum_at_owner(partial_value.astype(jnp.bfloat16), "tp", 1)
    stream_cols = (
        lax.dynamic_slice_in_dim(resid, column_first, columns, 1).astype(jnp.float32) + mixed_sum
    )
    square_sum = of_everyone(jnp.sum(stream_cols * stream_cols, axis=1, keepdims=True), "tp")
    gain_cols = lax.dynamic_slice_in_dim(norm_gain, column_first, columns, 0)
    normed = (stream_cols * lax.rsqrt(square_sum / model_width + epsilon) * gain_cols).astype(
        jnp.bfloat16
    )
    capacity = 5 * rows_here // (2 * sp_count)
    chosen = routes.reshape(-1)
    onehot = (chosen[:, None] == jnp.arange(sp_count, dtype=jnp.int32)[None, :]).astype(jnp.int32)
    before = jnp.cumsum(onehot, axis=0) - onehot
    rank_within = jnp.sum(before * onehot, axis=1)
    slot_index = chosen * capacity + rank_within
    source_row = (
        jnp.zeros((sp_count * capacity,), jnp.int32)
        .at[slot_index]
        .set(jnp.arange(chosen.shape[0], dtype=jnp.int32) // routes.shape[1])
    )
    filled = jnp.zeros((sp_count * capacity,), jnp.bool_).at[slot_index].set(True)
    outgoing = jnp.where(filled[:, None], normed[source_row], jnp.zeros((), jnp.bfloat16))
    outgoing = outgoing.reshape(sp_count, capacity, normed.shape[1])
    gate_here = gate_weight[0]
    up_here = up_weight[0]
    local_down_weight = down_weight[0]
    arrived = lax.all_to_all(outgoing, "sp", split_axis=0, concat_axis=0, tiled=True)
    arrived_rows = arrived.reshape(-1, columns)
    col_part = lax.all_gather(arrived_rows, "tp", axis=1, tiled=True)
    gate_sum = jnp.dot(col_part, gate_here, preferred_element_type=jnp.float32)
    up_sum = jnp.dot(col_part, up_here, preferred_element_type=jnp.float32)
    slot_shape = arrived.shape
    hidden = (jax.nn.silu(gate_sum) * up_sum).astype(jnp.bfloat16)
    partial_term = jnp.dot(hidden, local_down_weight, preferred_element_type=jnp.float32)
    expert_rows = sum_at_owner(partial_term.astype(jnp.bfloat16), "tp", 1).astype(jnp.bfloat16)
    returned = expert_rows.reshape(slot_shape[0], slot_shape[1], columns)
    returned_back = lax.all_to_all(returned, "sp", split_axis=0, concat_axis=0, tiled=True)
    returned_flat = returned_back.reshape(sp_count * capacity, columns)
    picked = (
        returned_flat[slot_index].reshape(rows_here, routes.shape[1], columns).astype(jnp.float32)
    )
    combined = jnp.sum(picked * route_weight[..., None], axis=1)
    return (stream_cols + combined).astype(jnp.bfloat16)


def solution(mesh):
    return jax.shard_map(
        local,
        mesh=mesh,
        in_specs=(
            P("sp", "tp"),
            P("sp", "tp"),
            P("sp", "tp"),
            P("tp", None),
            P("tp", None),
            P("sp", None),
            P(),
            P("sp", None),
            P("sp", None),
            P("sp", None, "tp"),
            P("sp", None, "tp"),
            P("sp", "tp", None),
        ),
        out_specs=P("sp", "tp"),
        check_vma=False,
    )
```

profile of v0, /device:TPU:1, one launch (start us, length us, event | category | flops | bytes accessed | tf_op | source)
XLA Modules:
  0.0 370.9 jit_solution(9054272636798588638)
XLA Ops:
  9.1 86.0 %all-gather.3.cloned.1.call-done = bf16[8192,128]{1,0:T(8,128)(2,1)} async-done(((bf16[256,128]{1,0:T(8,128)(2,1)}), bf16[8192,128]{1,0:T(8,128)(2,1)}) %all-gather.3.cloned.1.call-update) | async-done | bytes 2097168 | tf_op jit(solution)/shard_map/all_gather | solution.py:17
  95.1 49.2 %conditional.1 = (f32[1,256]{1,0:T(1,128)}, f32[1,256,64]{1,2,0:T(8,128)}) conditional(s32[]{:T(128)} %convert_element_type.51, () %tuple.31, (bf16[8192,128]{1,0:T(8,128)(2,1)}, bf16[256,64]{0,1:T(8,128)(2,1)}, s32[]{:T(128)}, f32[1,8192]{1,0:T(1,128)}) %tuple.32), branch_computations={%region_0.0_spmd, %region_1.6_spmd} | conditional | flops 70830592 | bytes 8277405 | solution.py:121
  95.9 5.0 %fusion.45 = (bf16[8192,64]{1,0:T(8,128)(2,1)}, bf16[8192,64]{1,0:T(8,128)(2,1)}) fusion(bf16[8192,128]{1,0:T(8,128)(2,1)} %get-tuple-element.217), kind=kLoop, calls=%fused_computation.87 | loop fusion | bytes 4194304 | tf_op jit(solution)/shard_map/split | solution.py:17
  101.0 43.3 %while.20 = (s32[]{:T(128)}, f32[1,256]{1,0:T(1,128)S(1)}, f32[1,256]{1,0:T(1,128)}, f32[1,256,64]{1,2,0:T(8,128)}, s32[]{:T(128)}, /*index=5*/bf16[8192,64]{1,0...) while((s32[]{:T(128)}, f32[1,256]{1,0:T(1,128)S(1)}, ...), condition=%wide.region_5.5_spmd.clone, body=%wide.region_2.4_spmd.clone.sunk | while | flops 70830592 | bytes 3884243 | solution.py:119
  103.9 2.0 fusion.62
  109.3 2.0 fusion.62
  114.8 2.0 fusion.62
  125.8 2.0 fusion.62
  136.8 2.0 fusion.62
  146.8 12.3 %all-to-all-start = ((bf16[16,256,128]{2,1,0:T(8,128)(2,1)}), bf16[16,256,128]{2,1,0:T(8,128)(2,1)S(1)}, u32[]{:S(2)}, u32[]{:S(2)}) async-start(bf16[16,256,128]{2,1,0:T(8,128)(2,1)} %bitcast.74), calls=%async_computation | async-start | bytes 2097152 | tf_op jit(solution)/shard_map/all_to_all | solution.py:27
  161.5 2.4 scatter_custom_fusion.1
  164.0 23.2 %all-to-all-done = bf16[16,256,128]{2,1,0:T(8,128)(2,1)S(1)} async-done(((bf16[16,256,128]{2,1,0:T(8,128)(2,1)}), bf16[16,256,128]{2,1,0:T(8,128)(2,1)S(1)}, u32[]{:S(2)}, u32[]{:S(2)}) %all-to-all-start) | async-done | bytes 1048608 | tf_op jit(solution)/shard_map/all_to_all | solution.py:27
  188.9 3.4 all-to-all-start.1
  193.2 2.4 scatter_custom_fusion
  195.7 3.9 %all-to-all-done.1 = f32[16,256,1]{1,2,0:T(1,128)S(1)} async-done(((f32[16,256,1]{1,2,0:T(1,128)}), f32[16,256,1]{1,2,0:T(1,128)S(1)}, u32[]{:S(2)}, u32[]{:S(2)}) %all-to-all-start.1) | async-done | bytes 16416 | tf_op jit(solution)/shard_map/all_to_all | solution.py:33
  202.9 15.5 %all_to_all.25 = bf16[32,20,128]{2,1,0:T(8,128)(2,1)S(1)} all-to-all(bf16[32,20,128]{2,1,0:T(8,128)(2,1)S(1)} %broadcast_select_fusion.2), channel_id=1, replica_groups=mesh['sp'=32,'tp'=16] {'sp'}, dimensions={0} | all-to-all | bytes 327680 | tf_op jit(solution)/shard_map/all_to_all | solution.py:156
  219.1 38.1 %all-gather.5.cloned.1.call-done = bf16[640,2048]{1,0:T(8,128)(2,1)} async-done(((bf16[640,128]{1,0:T(8,128)(2,1)}), bf16[640,2048]{1,0:T(8,128)(2,1)}) %all-gather.5.cloned.1.call-update) | async-done | bytes 2621456 | tf_op jit(solution)/shard_map/all_gather | solution.py:158
  257.2 3.4 fusion.26
  260.7 6.2 %fusion.21 = bf16[80,16,8,128]{3,2,1,0:T(8,128)(2,1)} fusion(bf16[1,256,2048]{2,1,0:T(8,128)(2,1)S(1)} %copy-done, bf16[640,2048]{1,0:T(8,128)(2,1)} %all-gather.5.cloned.1.call-done, bf16[1,2048,256]{2,1,0:T(8,128)(2,1)S(1)} %copy-done.6, f32[640,256]{1,0:T(8,128)} %fusion.26), kind=kOutput, calls=%fused_computation.40 | convolution fusion | flops 1344471040 | bytes 7995392 | tf_op jit(solution)/shard_map/dot_general | solution.py:163
  266.9 2.4 copy.43
  269.3 67.0 %all_to_all.26 = bf16[16,640,128]{2,1,0:T(8,128)(2,1)} all-to-all(bf16[16,640,128]{2,1,0:T(8,128)(2,1)S(1)} %bitcast.91), channel_id=1, replica_groups=mesh['sp'=32,'tp'=16] {'tp'}, dimensions={0} | all-to-all | bytes 5242880 | tf_op jit(solution)/shard_map/all_to_all | solution.py:27
  336.3 2.1 reduce_sum.77
  339.2 9.9 %all-to-all-start.4 = ((bf16[32,20,128]{2,1,0:T(8,128)(2,1)}), bf16[32,20,128]{2,1,0:T(8,128)(2,1)S(1)}, u32[]{:S(2)}, u32[]{:S(2)}) async-start(bf16[32,20,128]{2,1,0:T(8,128)(2,1)} %reshape.156), calls=%async_computation.4 | async-start | bytes 393216 | tf_op jit(solution)/shard_map/all_to_all | solution.py:166
  349.3 11.5 %all-to-all-done.4 = bf16[32,20,128]{2,1,0:T(8,128)(2,1)S(1)} async-done(((bf16[32,20,128]{2,1,0:T(8,128)(2,1)}), bf16[32,20,128]{2,1,0:T(8,128)(2,1)S(1)}, u32[]{:S(2)}, u32[]{:S(2)}) %all-to-all-start.4) | async-done | bytes 163872 | tf_op jit(solution)/shard_map/all_to_all | solution.py:166
  (131 shorter events, 52.0 us)
Async XLA Ops:
  6.5 254.1 %copy-start = (bf16[1,256,2048]{2,1,0:T(8,128)(2,1)S(1)}, bf16[1,256,2048]{2,1,0:T(8,128)(2,1)}, u32[]{:S(2)}) copy-start(bf16[1,256,2048]{2,1,0:T(8,128)(2,1)} %param.27) | copy-start | bytes 3145732
  6.5 88.6 %all-gather.3.cloned.1.call-start = ((), (), s32[]{:S(2)}) async-start(), calls=%async_computation.5 | async-start | bytes 2162688 | tf_op jit(solution)/shard_map/all_gather | solution.py:17
  95.1 49.2 %copy-start.1 = (bf16[64,2048]{1,0:T(8,128)(2,1)S(1)}, bf16[64,2048]{1,0:T(8,128)(2,1)}, u32[]{:S(2)}) copy-start(bf16[64,2048]{1,0:T(8,128)(2,1)} %param.20) | copy-start | bytes 786436
  95.9 5.0 %copy-start.2 = (bf16[256,64]{0,1:T(8,128)(2,1)S(1)}, bf16[256,64]{0,1:T(8,128)(2,1)}, u32[]{:S(2)}) copy-start(bf16[256,64]{0,1:T(8,128)(2,1)} %get-tuple-element.272) | copy-start | bytes 98308 | tf_op jit(solution)/shard_map/cond
  144.3 14.9 %copy-start.3 = (s32[256,2]{0,1:T(2,128)S(1)}, s32[256,2]{0,1:T(2,128)}, u32[]{:S(2)}) copy-start(s32[256,2]{0,1:T(2,128)} %param.23) | copy-start | bytes 6148
  146.8 40.3 %all-to-all-start = ((bf16[16,256,128]{2,1,0:T(8,128)(2,1)}), bf16[16,256,128]{2,1,0:T(8,128)(2,1)S(1)}, u32[]{:S(2)}, u32[]{:S(2)}) async-start(bf16[16,256,128]{2,1,0:T(8,128)(2,1)} %bitcast.74), calls=%async_computation | async-start | bytes 2097152 | tf_op jit(solution)/shard_map/all_to_all | solution.py:27
  161.1 96.1 %copy-start.5 = (bf16[1,2048,256]{2,1,0:T(8,128)(2,1)S(1)}, bf16[1,2048,256]{2,1,0:T(8,128)(2,1)}, u32[]{:S(2)}) copy-start(bf16[1,2048,256]{2,1,0:T(8,128)(2,1)} %param.25) | copy-start | bytes 3145732
  188.9 10.8 %all-to-all-start.1 = ((f32[16,256,1]{1,2,0:T(1,128)}), f32[16,256,1]{1,2,0:T(1,128)S(1)}, u32[]{:S(2)}, u32[]{:S(2)}) async-start(f32[16,256,1]{1,2,0:T(1,128)} %broadcast_in_dim.90), calls=%async_computation.1 | async-start | bytes 32768 | tf_op jit(solution)/shard_map/all_to_all | solution.py:33
  192.3 64.9 %all-gather.5.cloned.1.call-start = ((), (), s32[]{:S(2)}) async-start(), calls=%async_computation.6 | async-start | bytes 2785280 | tf_op jit(solution)/shard_map/all_gather | solution.py:158
  219.1 41.5 %copy-start.6 = (bf16[1,2048,256]{2,1,0:T(8,128)(2,1)S(1)}, bf16[1,2048,256]{2,1,0:T(8,128)(2,1)}, u32[]{:S(2)}) copy-start(bf16[1,2048,256]{2,1,0:T(8,128)(2,1)} %param.26) | copy-start | bytes 3145732
  336.3 12.8 %copy-start.4 = (f32[256,2]{0,1:T(2,128)S(1)}, f32[256,2]{0,1:T(2,128)}, u32[]{:S(2)}) copy-start(f32[256,2]{0,1:T(2,128)} %param.24) | copy-start | bytes 6148
  339.2 21.5 %all-to-all-start.4 = ((bf16[32,20,128]{2,1,0:T(8,128)(2,1)}), bf16[32,20,128]{2,1,0:T(8,128)(2,1)S(1)}, u32[]{:S(2)}, u32[]{:S(2)}) async-start(bf16[32,20,128]{2,1,0:T(8,128)(2,1)} %reshape.156), calls=%async_computation.4 | async-start | bytes 393216 | tf_op jit(solution)/shard_map/all_to_all | solution.py:166
Sparse Core Ops, SparseCore 0:
  10.5 84.5 all-gather.2
  219.2 37.9 all-gather.4
where the time goes:
time: 372 us; the launch traced here: 371 us
  waiting for transfers between devices  163 us (44%)
  blocking collectives  82.6 us (22%)
  matrix products  38 us (10%)
  local copies, waits for them, and re-layouts  29.2 us (8%)
  starting transfers between devices  25.7 us (7%)
  other arithmetic  19 us (5%)
  between operations  13.6 us (4%)
    all_gather x1, waiting for transfers between devices, in_one_piece(): lax.all_gather(both, axis, axis=dim, tiled=True)  86 us
    all_to_all x1, blocking collectives, sum_at_owner(): lax.all_to_all(tiles, axis, split_axis=0, concat_axis=0, tiled=True)  67 us
    all_gather x1, waiting for transfers between devices, local(): col_part = lax.all_gather(arrived_rows, 'tp', axis=1, tiled=True)  38.1 us
    all_to_all x1, waiting for transfers between devices, sum_at_owner(): lax.all_to_all(tiles, axis, split_axis=0, concat_axis=0, tiled=True)  23.2 us
    dot_general x8, matrix products, attend_block(): jnp.einsum('hqk,hkd->hqd', weights.astype(jnp.bfloat16), value_rows, pref...  16.2 us
    all_to_all x1, blocking collectives, local(): lax.all_to_all(outgoing, 'sp', split_axis=0, concat_axis=0, tiled=True)  15.5 us
    all_to_all x1, starting transfers between devices, sum_at_owner(): lax.all_to_all(tiles, axis, split_axis=0, concat_axis=0, tiled=True)  12.3 us
    all_to_all x1, waiting for transfers between devices, local(): lax.all_to_all(returned, 'sp', split_axis=0, concat_axis=0, tiled=True)  11.5 us
  transfers between devices with their start and end apart: 5, of which 5 were waited for; matrix products, arithmetic and copies ran while one was open for 2% of the time, Pallas kernels for 0%

commit v1 on v0

--- a/solution.py
+++ b/solution.py
@@ -1,3 +1,4 @@
+import functools
 import math
 import jax
 import jax.numpy as jnp
@@ -6,6 +7,38 @@
 
 HD = 64
 epsilon = 1e-06
+
+
+def store_the_weights(my_data, pos_dim):
+    my_data = jnp.moveaxis(my_data, 0, pos_dim)
+    v_next = my_data.shape
+    return my_data.reshape(
+        *v_next[:pos_dim], v_next[pos_dim] * v_next[pos_dim + 1], *v_next[pos_dim + 2 :]
+    )
+
+
+def switch_digits(mat, shard_axis, dim_k):
+    many = lax.axis_size(shard_axis)
+    pile = [(m, (m + 1) % many) for m in range(many)]
+    all_rows = [(c, dd) for dd, c in pile]
+    big, block_next = ([], [])
+    for k in [*range(many - 1)]:
+        if k % 2 == 0:
+            far_arr = lax.ppermute(big[-1] if big else mat, shard_axis, pile)
+            big.append(far_arr)
+        else:
+            block_next.append(
+                lax.ppermute(block_next[-1] if block_next else mat, shard_axis, perm=all_rows)
+            )
+    f_next = jnp.stack([*big[::-1], mat, *block_next])
+    d_next = lax.axis_index(shard_axis)
+    base_arr = len(big)
+    field_out = d_next - base_arr
+    f_next = f_next[(jnp.arange(many) - field_out) % many]
+    return store_the_weights(f_next, dim_k)
+
+
+advance_strings = functools.partial(switch_digits, shard_axis="tp", dim_k=1)
 
 
 def in_one_piece(arrays, axis, dim, along):
@@ -155,7 +188,7 @@
     local_down_weight = down_weight[0]
     arrived = lax.all_to_all(outgoing, "sp", split_axis=0, concat_axis=0, tiled=True)
     arrived_rows = arrived.reshape(-1, columns)
-    col_part = lax.all_gather(arrived_rows, "tp", axis=1, tiled=True)
+    col_part = advance_strings(arrived_rows)
     gate_sum = jnp.dot(col_part, gate_here, preferred_element_type=jnp.float32)
     up_sum = jnp.dot(col_part, up_here, preferred_element_type=jnp.float32)
     slot_shape = arrived.shape

time: 372 us -> 398 us (1.070)
  starting transfers between devices: 25.7 us -> 54.2 us
  waiting for transfers between devices: 163 us -> 135 us
  local copies, waits for them, and re-layouts: 29.2 us -> 49.8 us
    all_gather x1 -> x0, waiting for transfers between devices: 38.1 us -> none  [local(): col_part = lax.all_gather(arrived_rows, 'tp', axis=1, tiled=True)]
    ppermute x0 -> x15, starting transfers between devices: none -> 34.6 us  [the longest x7 25.5 us: switch_digits(): lax.ppermute(block_next[-1] if block_next else mat, shard_axis, perm=all_...]
    unnamed x16 -> x31, local copies, waits for them, and re-layouts: 2.13 us -> 14.1 us
    ppermute x0 -> x15, waiting for transfers between devices: none -> 10.3 us  [the longest x8 9.13 us: switch_digits(): far_arr = lax.ppermute(big[-1] if big else mat, shard_axis, pile)]
    all_to_all x1, starting transfers between devices: 9.9 us -> 3.86 us  [local(): lax.all_to_all(returned, 'sp', split_axis=0, concat_axis=0, tiled=True)]
    transpose x0 -> x1, local copies, waits for them, and re-layouts: none -> 4.48 us  [store_the_weights(): my_data = jnp.moveaxis(my_data, 0, pos_dim)]
    gather x0 -> x1, local copies, waits for them, and re-layouts: none -> 4.15 us  [switch_digits(): f_next = f_next[(jnp.arange(many) - field_out) % many]]
  transfers between devices with their start and end apart: 5 -> 19, of which waited for: 5 -> 17; matrix products, arithmetic and copies ran while one was open for 2% -> 5% of each run, Pallas kernels for 0% -> 0%
where the time goes in v1:
time: 398 us; the launch traced here: 396 us
  waiting for transfers between devices  135 us (34%)
  blocking collectives  86 us (22%)
  starting transfers between devices  54.2 us (14%)
  local copies, waits for them, and re-layouts  49.8 us (13%)
  matrix products  38.1 us (10%)
  other arithmetic  19.8 us (5%)
  between operations  13.7 us (3%)
    all_gather x1, waiting for transfers between devices, in_one_piece(): lax.all_gather(both, axis, axis=dim, tiled=True)  86 us
    all_to_all x1, blocking collectives, sum_at_owner(): lax.all_to_all(tiles, axis, split_axis=0, concat_axis=0, tiled=True)  70.4 us
    ppermute x7, starting transfers between devices, switch_digits(): lax.ppermute(block_next[-1] if block_next else mat, shard_axis, perm=all_...  25.5 us
    all_to_all x1, waiting for transfers between devices, sum_at_owner(): lax.all_to_all(tiles, axis, split_axis=0, concat_axis=0, tiled=True)  23.2 us
    dot_general x8, matrix products, attend_block(): jnp.einsum('hqk,hkd->hqd', weights.astype(jnp.bfloat16), value_rows, pref...  16.2 us
    all_to_all x1, blocking collectives, local(): lax.all_to_all(outgoing, 'sp', split_axis=0, concat_axis=0, tiled=True)  15.5 us
    unnamed x31, local copies, waits for them, and re-layouts  14.1 us
    all_to_all x1, starting transfers between devices, sum_at_owner(): lax.all_to_all(tiles, axis, split_axis=0, concat_axis=0, tiled=True)  12.4 us
  transfers between devices with their start and end apart: 19, of which 17 were waited for; matrix products, arithmetic and copies ran while one was open for 5% of the time, Pallas kernels for 0%

profile of v1, /device:TPU:1, one launch (start us, length us, event | category | flops | bytes accessed | tf_op | source)
XLA Modules:
  0.0 396.4 jit_solution(5875811501392070888)
XLA Ops:
  9.1 86.0 %all-gather.2.cloned.1.call-done = bf16[8192,128]{1,0:T(8,128)(2,1)} async-done(((bf16[256,128]{1,0:T(8,128)(2,1)}), bf16[8192,128]{1,0:T(8,128)(2,1)}) %all-gather.2.cloned.1.call-update) | async-done | bytes 2097168 | tf_op jit(solution)/shard_map/all_gather | solution.py:50
  95.1 50.0 %conditional.1 = (f32[1,256]{1,0:T(1,128)}, f32[1,256,64]{1,2,0:T(8,128)}) conditional(s32[]{:T(128)} %convert_element_type.51, () %tuple.31, (bf16[8192,128]{1,0:T(8,128)(2,1)}, bf16[256,64]{0,1:T(8,128)(2,1)}, s32[]{:T(128)}, f32[1,8192]{1,0:T(1,128)}) %tuple.32), branch_computations={%region_0.0_spmd, %region_1.6_spmd} | conditional | flops 70830592 | bytes 8277405 | solution.py:154
  95.9 5.0 %fusion.47 = (bf16[8192,64]{1,0:T(8,128)(2,1)}, bf16[8192,64]{1,0:T(8,128)(2,1)}) fusion(bf16[8192,128]{1,0:T(8,128)(2,1)} %get-tuple-element.217), kind=kLoop, calls=%fused_computation.111 | loop fusion | bytes 4194304 | tf_op jit(solution)/shard_map/split | solution.py:50
  101.0 44.1 %while.20 = (s32[]{:T(128)}, f32[1,256]{1,0:T(1,128)S(1)}, f32[1,256]{1,0:T(1,128)}, f32[1,256,64]{1,2,0:T(8,128)}, s32[]{:T(128)}, /*index=5*/bf16[8192,64]{1,0...) while((s32[]{:T(128)}, f32[1,256]{1,0:T(1,128)S(1)}, ...), condition=%wide.region_5.5_spmd.clone, body=%wide.region_2.4_spmd.clone.sunk | while | flops 70830592 | bytes 3884243 | solution.py:152
  147.7 12.4 %all-to-all-start = ((bf16[16,256,128]{2,1,0:T(8,128)(2,1)}), bf16[16,256,128]{2,1,0:T(8,128)(2,1)S(1)}, u32[]{:S(2)}, u32[]{:S(2)}) async-start(bf16[16,256,128]{2,1,0:T(8,128)(2,1)} %bitcast.108), calls=%async_computation | async-start | bytes 2097152 | tf_op jit(solution)/shard_map/all_to_all | solution.py:60
  162.4 2.4 scatter_custom_fusion.1
  164.8 23.2 %all-to-all-done = bf16[16,256,128]{2,1,0:T(8,128)(2,1)S(1)} async-done(((bf16[16,256,128]{2,1,0:T(8,128)(2,1)}), bf16[16,256,128]{2,1,0:T(8,128)(2,1)S(1)}, u32[]{:S(2)}, u32[]{:S(2)}) %all-to-all-start) | async-done | bytes 1048608 | tf_op jit(solution)/shard_map/all_to_all | solution.py:60
  189.8 3.4 all-to-all-start.1
  196.5 4.0 %all-to-all-done.1 = f32[16,256,1]{1,2,0:T(1,128)S(1)} async-done(((f32[16,256,1]{1,2,0:T(1,128)}), f32[16,256,1]{1,2,0:T(1,128)S(1)}, u32[]{:S(2)}, u32[]{:S(2)}) %all-to-all-start.1) | async-done | bytes 16416 | tf_op jit(solution)/shard_map/all_to_all | solution.py:66
  203.7 15.5 %all_to_all.25 = bf16[32,20,128]{2,1,0:T(8,128)(2,1)S(1)} all-to-all(bf16[32,20,128]{2,1,0:T(8,128)(2,1)S(1)} %broadcast_select_fusion.2), channel_id=1, replica_groups=mesh['sp'=32,'tp'=16] {'sp'}, dimensions={0} | all-to-all | bytes 327680 | tf_op jit(solution)/shard_map/all_to_all | solution.py:189
  223.7 2.5 collective-permute-start.1
  228.4 2.5 collective-permute-start.2
  235.9 3.2 collective-permute-start.10
  240.7 4.4 %collective-permute-start.11 = (bf16[640,128]{1,0:T(8,128)(2,1)S(1)}, bf16[640,128]{1,0:T(8,128)(2,1)S(1)}, u32[]{:S(2)}, u32[]{:S(2)}) collective-permute-start(bf16[640,128]{1,0:T(8,128)(2,1)S(1)} %collective-permute-done.10), channel_id=1, source_target_pairs={{1,0},{2,1},{3,2},{4,3},{5,4},{6,5},{7,6},{8,7},{9,8},{10,9},{11,1... | collective-permute-start | bytes 491528 | tf_op jit(solution)/shard_map/ppermute | solution.py:31
  246.1 4.9 %collective-permute-start.12 = (bf16[640,128]{1,0:T(8,128)(2,1)S(1)}, bf16[640,128]{1,0:T(8,128)(2,1)S(1)}, u32[]{:S(2)}, u32[]{:S(2)}) collective-permute-start(bf16[640,128]{1,0:T(8,128)(2,1)S(1)} %collective-permute-done.11), channel_id=1, source_target_pairs={{1,0},{2,1},{3,2},{4,3},{5,4},{6,5},{7,6},{8,7},{9,8},{10,9},{11,1... | collective-permute-start | bytes 491528 | tf_op jit(solution)/shard_map/ppermute | solution.py:31
  252.1 4.9 %collective-permute-start.13 = (bf16[640,128]{1,0:T(8,128)(2,1)S(1)}, bf16[640,128]{1,0:T(8,128)(2,1)S(1)}, u32[]{:S(2)}, u32[]{:S(2)}) collective-permute-start(bf16[640,128]{1,0:T(8,128)(2,1)S(1)} %collective-permute-done.12), channel_id=1, source_target_pairs={{1,0},{2,1},{3,2},{4,3},{5,4},{6,5},{7,6},{8,7},{9,8},{10,9},{11,1... | collective-permute-start | bytes 491528 | tf_op jit(solution)/shard_map/ppermute | solution.py:31
  258.1 5.1 %collective-permute-start.14 = (bf16[640,128]{1,0:T(8,128)(2,1)S(1)}, bf16[640,128]{1,0:T(8,128)(2,1)S(1)}, u32[]{:S(2)}, u32[]{:S(2)}) collective-permute-start(bf16[640,128]{1,0:T(8,128)(2,1)S(1)} %collective-permute-done.13), channel_id=1, source_target_pairs={{1,0},{2,1},{3,2},{4,3},{5,4},{6,5},{7,6},{8,7},{9,8},{10,9},{11,1... | collective-permute-start | bytes 491528 | tf_op jit(solution)/shard_map/ppermute | solution.py:31
  276.9 4.1 %gather_fusion.1 = bf16[16,640,128]{2,1,0:T(8,128)(2,1)} fusion(bf16[16,640,128]{2,1,0:T(8,128)(2,1)} %bitcast_dynamic-update-slice_fusion, s32[1024]{0:T(1024)S(1)} %pad_clamp_fusion.1), kind=kCustom, calls=%fused_computation.1 | custom fusion | bytes 5242944 | tf_op jit(solution)/shard_map/gather | solution.py:37
  281.1 4.5 %copy.36 = bf16[640,16,128]{0,2,1:T(8,128)(2,1)} copy(bf16[640,16,128]{2,0,1:T(8,128)(2,1)} %bitcast.125) | data formatting | bytes 5242880 | tf_op jit(solution)/shard_map/transpose | solution.py:13
  285.5 3.6 fusion.26
  289.1 6.2 %fusion.21 = bf16[80,16,8,128]{3,2,1,0:T(8,128)(2,1)} fusion(bf16[1,256,2048]{2,1,0:T(8,128)(2,1)S(1)} %copy-done, bf16[640,2048]{0,1:T(8,128)(2,1)} %bitcast.128, bf16[1,2048,256]{2,1,0:T(8,128)(2,1)S(1)} %copy-done.6, f32[640,256]{1,0:T(8,128)} %fusion.26), kind=kOutput, calls=%fused_computation.41 | convolution fusion | flops 1344471040 | bytes 7995392 | tf_op jit(solution)/shard_map/dot_general | solution.py:196
  297.8 70.4 %all_to_all.26 = bf16[16,640,128]{2,1,0:T(8,128)(2,1)} all-to-all(bf16[16,640,128]{2,1,0:T(8,128)(2,1)S(1)} %bitcast.126), channel_id=1, replica_groups=mesh['sp'=32,'tp'=16] {'tp'}, dimensions={0} | all-to-all | bytes 5242880 | tf_op jit(solution)/shard_map/all_to_all | solution.py:60
  371.1 3.9 all-to-all-start.4
  375.1 11.1 %all-to-all-done.4 = bf16[32,20,128]{2,1,0:T(8,128)(2,1)S(1)} async-done(((bf16[32,20,128]{2,1,0:T(8,128)(2,1)}), bf16[32,20,128]{2,1,0:T(8,128)(2,1)S(1)}, u32[]{:S(2)}, u32[]{:S(2)}) %all-to-all-start.4) | async-done | bytes 163872 | tf_op jit(solution)/shard_map/all_to_all | solution.py:199
  (179 shorter events, 99.4 us)
Async XLA Ops:
  6.5 282.6 %copy-start = (bf16[1,256,2048]{2,1,0:T(8,128)(2,1)S(1)}, bf16[1,256,2048]{2,1,0:T(8,128)(2,1)}, u32[]{:S(2)}) copy-start(bf16[1,256,2048]{2,1,0:T(8,128)(2,1)} %param.27) | copy-start | bytes 3145732
  6.5 88.6 %all-gather.2.cloned.1.call-start = ((), (), s32[]{:S(2)}) async-start(), calls=%async_computation.5 | async-start | bytes 2162688 | tf_op jit(solution)/shard_map/all_gather | solution.py:50
  95.1 50.0 %copy-start.1 = (bf16[64,2048]{1,0:T(8,128)(2,1)S(1)}, bf16[64,2048]{1,0:T(8,128)(2,1)}, u32[]{:S(2)}) copy-start(bf16[64,2048]{1,0:T(8,128)(2,1)} %param.20) | copy-start | bytes 786436
  95.9 5.0 %copy-start.2 = (bf16[256,64]{0,1:T(8,128)(2,1)S(1)}, bf16[256,64]{0,1:T(8,128)(2,1)}, u32[]{:S(2)}) copy-start(bf16[256,64]{0,1:T(8,128)(2,1)} %get-tuple-element.272) | copy-start | bytes 98308 | tf_op jit(solution)/shard_map/cond
  145.1 14.9 %copy-start.3 = (s32[256,2]{0,1:T(2,128)S(1)}, s32[256,2]{0,1:T(2,128)}, u32[]{:S(2)}) copy-start(s32[256,2]{0,1:T(2,128)} %param.23) | copy-start | bytes 6148
  147.7 40.4 %all-to-all-start = ((bf16[16,256,128]{2,1,0:T(8,128)(2,1)}), bf16[16,256,128]{2,1,0:T(8,128)(2,1)S(1)}, u32[]{:S(2)}, u32[]{:S(2)}) async-start(bf16[16,256,128]{2,1,0:T(8,128)(2,1)} %bitcast.108), calls=%async_computation | async-start | bytes 2097152 | tf_op jit(solution)/shard_map/all_to_all | solution.py:60
  189.8 10.8 %all-to-all-start.1 = ((f32[16,256,1]{1,2,0:T(1,128)}), f32[16,256,1]{1,2,0:T(1,128)S(1)}, u32[]{:S(2)}, u32[]{:S(2)}) async-start(f32[16,256,1]{1,2,0:T(1,128)} %broadcast_in_dim.91), calls=%async_computation.1 | async-start | bytes 32768 | tf_op jit(solution)/shard_map/all_to_all | solution.py:66
  219.3 4.4 %collective-permute-start = (bf16[640,128]{1,0:T(8,128)(2,1)S(1)}, bf16[640,128]{1,0:T(8,128)(2,1)S(1)}, u32[]{:S(2)}, u32[]{:S(2)}) collective-permute-start(bf16[640,128]{1,0:T(8,128)(2,1)S(1)} %reshape.206), channel_id=1, source_target_pairs={{0,1},{1,2},{2,3},{3,4},{4,5},{5,6},{6,7},{7,8},{8,9},{9,10},{10,1... | collective-permute-start | bytes 491528 | tf_op jit(solution)/shard_map/ppermute | solution.py:27
  223.7 4.7 %collective-permute-start.1 = (bf16[640,128]{1,0:T(8,128)(2,1)S(1)}, bf16[640,128]{1,0:T(8,128)(2,1)S(1)}, u32[]{:S(2)}, u32[]{:S(2)}) collective-permute-start(bf16[640,128]{1,0:T(8,128)(2,1)S(1)} %collective-permute-done), channel_id=1, source_target_pairs={{0,1},{1,2},{2,3},{3,4},{4,5},{5,6},{6,7},{7,8},{8,9},{9,10},{10,1... | collective-permute-start | bytes 491528 | tf_op jit(solution)/shard_map/ppermute | solution.py:27
  226.1 5.0 %collective-permute-start.8 = (bf16[640,128]{1,0:T(8,128)(2,1)S(1)}, bf16[640,128]{1,0:T(8,128)(2,1)S(1)}, u32[]{:S(2)}, u32[]{:S(2)}) collective-permute-start(bf16[640,128]{1,0:T(8,128)(2,1)S(1)} %reshape.206), channel_id=1, source_target_pairs={{1,0},{2,1},{3,2},{4,3},{5,4},{6,5},{7,6},{8,7},{9,8},{10,9},{11,1... | collective-permute-start | bytes 491528 | tf_op jit(solution)/shard_map/ppermute | solution.py:31
  228.4 5.6 %collective-permute-start.2 = (bf16[640,128]{1,0:T(8,128)(2,1)S(1)}, bf16[640,128]{1,0:T(8,128)(2,1)S(1)}, u32[]{:S(2)}, u32[]{:S(2)}) collective-permute-start(bf16[640,128]{1,0:T(8,128)(2,1)S(1)} %collective-permute-done.1), channel_id=1, source_target_pairs={{0,1},{1,2},{2,3},{3,4},{4,5},{5,6},{6,7},{7,8},{8,9},{9,10},{10,1... | collective-permute-start | bytes 491528 | tf_op jit(solution)/shard_map/ppermute | solution.py:27
  231.2 4.7 %collective-permute-start.9 = (bf16[640,128]{1,0:T(8,128)(2,1)S(1)}, bf16[640,128]{1,0:T(8,128)(2,1)S(1)}, u32[]{:S(2)}, u32[]{:S(2)}) collective-permute-start(bf16[640,128]{1,0:T(8,128)(2,1)S(1)} %collective-permute-done.8), channel_id=1, source_target_pairs={{1,0},{2,1},{3,2},{4,3},{5,4},{6,5},{7,6},{8,7},{9,8},{10,9},{11,1... | collective-permute-start | bytes 491528 | tf_op jit(solution)/shard_map/ppermute | solution.py:31
  234.0 6.0 %collective-permute-start.3 = (bf16[640,128]{1,0:T(8,128)(2,1)S(1)}, bf16[640,128]{1,0:T(8,128)(2,1)S(1)}, u32[]{:S(2)}, u32[]{:S(2)}) collective-permute-start(bf16[640,128]{1,0:T(8,128)(2,1)S(1)} %collective-permute-done.2), channel_id=1, source_target_pairs={{0,1},{1,2},{2,3},{3,4},{4,5},{5,6},{6,7},{7,8},{8,9},{9,10},{10,1... | collective-permute-start | bytes 491528 | tf_op jit(solution)/shard_map/ppermute | solution.py:27
  235.9 4.7 %collective-permute-start.10 = (bf16[640,128]{1,0:T(8,128)(2,1)S(1)}, bf16[640,128]{1,0:T(8,128)(2,1)S(1)}, u32[]{:S(2)}, u32[]{:S(2)}) collective-permute-start(bf16[640,128]{1,0:T(8,128)(2,1)S(1)} %collective-permute-done.9), channel_id=1, source_target_pairs={{1,0},{2,1},{3,2},{4,3},{5,4},{6,5},{7,6},{8,7},{9,8},{10,9},{11,1... | collective-permute-start | bytes 491528 | tf_op jit(solution)/shard_map/ppermute | solution.py:31
  240.0 6.0 %collective-permute-start.4 = (bf16[640,128]{1,0:T(8,128)(2,1)S(1)}, bf16[640,128]{1,0:T(8,128)(2,1)S(1)}, u32[]{:S(2)}, u32[]{:S(2)}) collective-permute-start(bf16[640,128]{1,0:T(8,128)(2,1)S(1)} %collective-permute-done.3), channel_id=1, source_target_pairs={{0,1},{1,2},{2,3},{3,4},{4,5},{5,6},{6,7},{7,8},{8,9},{9,10},{10,1... | collective-permute-start | bytes 491528 | tf_op jit(solution)/shard_map/ppermute | solution.py:27
  240.7 5.4 %collective-permute-start.11 = (bf16[640,128]{1,0:T(8,128)(2,1)S(1)}, bf16[640,128]{1,0:T(8,128)(2,1)S(1)}, u32[]{:S(2)}, u32[]{:S(2)}) collective-permute-start(bf16[640,128]{1,0:T(8,128)(2,1)S(1)} %collective-permute-done.10), channel_id=1, source_target_pairs={{1,0},{2,1},{3,2},{4,3},{5,4},{6,5},{7,6},{8,7},{9,8},{10,9},{11,1... | collective-permute-start | bytes 491528 | tf_op jit(solution)/shard_map/ppermute | solution.py:31
  246.0 6.0 %collective-permute-start.5 = (bf16[640,128]{1,0:T(8,128)(2,1)S(1)}, bf16[640,128]{1,0:T(8,128)(2,1)S(1)}, u32[]{:S(2)}, u32[]{:S(2)}) collective-permute-start(bf16[640,128]{1,0:T(8,128)(2,1)S(1)} %collective-permute-done.4), channel_id=1, source_target_pairs={{0,1},{1,2},{2,3},{3,4},{4,5},{5,6},{6,7},{7,8},{8,9},{9,10},{10,1... | collective-permute-start | bytes 491528 | tf_op jit(solution)/shard_map/ppermute | solution.py:27
  246.1 6.0 %collective-permute-start.12 = (bf16[640,128]{1,0:T(8,128)(2,1)S(1)}, bf16[640,128]{1,0:T(8,128)(2,1)S(1)}, u32[]{:S(2)}, u32[]{:S(2)}) collective-permute-start(bf16[640,128]{1,0:T(8,128)(2,1)S(1)} %collective-permute-done.11), channel_id=1, source_target_pairs={{1,0},{2,1},{3,2},{4,3},{5,4},{6,5},{7,6},{8,7},{9,8},{10,9},{11,1... | collective-permute-start | bytes 491528 | tf_op jit(solution)/shard_map/ppermute | solution.py:31
  251.9 6.1 %collective-permute-start.6 = (bf16[640,128]{1,0:T(8,128)(2,1)S(1)}, bf16[640,128]{1,0:T(8,128)(2,1)}, u32[]{:S(2)}, u32[]{:S(2)}) collective-permute-start(bf16[640,128]{1,0:T(8,128)(2,1)S(1)} %collective-permute-done.5), channel_id=1, source_target_pairs={{0,1},{1,2},{2,3},{3,4},{4,5},{5,6},{6,7},{7,8},{8,9},{9,10},{10,1... | collective-permute-start | bytes 491528 | tf_op jit(solution)/shard_map/ppermute | solution.py:27
  252.1 6.0 %collective-permute-start.13 = (bf16[640,128]{1,0:T(8,128)(2,1)S(1)}, bf16[640,128]{1,0:T(8,128)(2,1)S(1)}, u32[]{:S(2)}, u32[]{:S(2)}) collective-permute-start(bf16[640,128]{1,0:T(8,128)(2,1)S(1)} %collective-permute-done.12), channel_id=1, source_target_pairs={{1,0},{2,1},{3,2},{4,3},{5,4},{6,5},{7,6},{8,7},{9,8},{10,9},{11,1... | collective-permute-start | bytes 491528 | tf_op jit(solution)/shard_map/ppermute | solution.py:31
  258.0 6.3 %collective-permute-start.7 = (bf16[640,128]{1,0:T(8,128)(2,1)}, bf16[640,128]{1,0:T(8,128)(2,1)}, u32[]{:S(2)}, u32[]{:S(2)}) collective-permute-start(bf16[640,128]{1,0:T(8,128)(2,1)} %collective-permute-done.6), channel_id=1, source_target_pairs={{0,1},{1,2},{2,3},{3,4},{4,5},{5,6},{6,7},{7,8},{8,9},{9,10},{10,1... | collective-permute-start | bytes 491528 | tf_op jit(solution)/shard_map/ppermute | solution.py:27
  258.1 18.1 %collective-permute-start.14 = (bf16[640,128]{1,0:T(8,128)(2,1)S(1)}, bf16[640,128]{1,0:T(8,128)(2,1)S(1)}, u32[]{:S(2)}, u32[]{:S(2)}) collective-permute-start(bf16[640,128]{1,0:T(8,128)(2,1)S(1)} %collective-permute-done.13), channel_id=1, source_target_pairs={{1,0},{2,1},{3,2},{4,3},{5,4},{6,5},{7,6},{8,7},{9,8},{10,9},{11,1... | collective-permute-start | bytes 491528 | tf_op jit(solution)/shard_map/ppermute | solution.py:31
  368.2 6.7 %copy-start.4 = (f32[256,2]{0,1:T(2,128)S(1)}, f32[256,2]{0,1:T(2,128)}, u32[]{:S(2)}) copy-start(f32[256,2]{0,1:T(2,128)} %param.24) | copy-start | bytes 6148
  371.1 15.1 %all-to-all-start.4 = ((bf16[32,20,128]{2,1,0:T(8,128)(2,1)}), bf16[32,20,128]{2,1,0:T(8,128)(2,1)S(1)}, u32[]{:S(2)}, u32[]{:S(2)}) async-start(bf16[32,20,128]{2,1,0:T(8,128)(2,1)} %reshape.209), calls=%async_computation.4 | async-start | bytes 393216 | tf_op jit(solution)/shard_map/all_to_all | solution.py:199
  (2 other events, 8.1 us)
Sparse Core Ops, SparseCore 0:
  10.5 84.5 all-gather.1
